TPU v7x, 128 devices: a whole 4x4x4 slice. The times are simulated.
128 devices in a mesh: rep: 2 (over z_hi), fs: 32 (over z_lo, y, x), tp: 2 (over core).
Axes of the slice: x: 4, y: 4, z: 4 (z_hi: 2, z_lo: 2; z = z_hi * 2 + z_lo), core: 2. Of those that a mesh axis runs over, the one named last changes fastest.
Arguments:
- tokens: bfloat16 [40960, 2048], P(('rep', 'fs', 'tp')), may hold values from -6 to 6
- mix_gain: float32 [2048], replicated, may hold values from 0.1 to 1.9
- w_bgate: bfloat16 [2048, 2048], P('fs', 'tp'), may hold values from -0.125 to 0.125
- w_cgate: bfloat16 [2048, 2048], P('fs', 'tp'), may hold values from -0.125 to 0.125
- w_value: bfloat16 [2048, 2048], P('fs', 'tp'), may hold values from -0.125 to 0.125
- conv_taps: float32 [3, 2048], replicated, may hold values from -3 to 3
- w_mixout: bfloat16 [2048, 2048], P('tp', 'fs'), may hold values from -0.125 to 0.125
- mlp_gain: float32 [2048], replicated, may hold values from 0.1 to 1.9
- w_gate: bfloat16 [2048, 2816], P('fs', 'tp'), may hold values from -0.125 to 0.125
- w_up: bfloat16 [2048, 2816], P('fs', 'tp'), may hold values from -0.125 to 0.125
- w_down: bfloat16 [2816, 2048], P('tp', 'fs'), may hold values from -0.109375 to 0.109375
Outputs:
- block_out: bfloat16 [40960, 2048], P(('rep', 'fs', 'tp'))
All inputs are finite; a program needn't handle non-finite values.
Results may differ from a plain program's by a relative error of at most 0.0085.
Values may be sent and summed in bfloat16 or wider, within the bound.
A program may use at most 128 MiB of HBM per device.

v0:
```python
import jax
import jax.numpy as jnp
from jax import lax
from jax.sharding import Mesh
from jax.sharding import PartitionSpec as P

FS = ("fs_0", "fs_1", "fs_2")
REP_FS_TP = ("rep", "fs_0", "fs_1", "fs_2", "tp")


def sent_to_all(array, axis):
    peers = lax.axis_size(axis)
    return lax.all_to_all(
        jnp.broadcast_to(array[None], (peers, *array.shape)), axis, 0, 0, tiled=True
    )


def in_order(blocks, dim):
    dims = list(blocks.shape[1:])
    dims[dim] *= blocks.shape[0]
    return jnp.moveaxis(blocks, 0, dim).reshape(dims)


def collect(array, axis, dim):
    blocks = sent_to_all(array, axis)
    return in_order(blocks, dim)


def stacked_from(array, axes, turns):
    blocks = array
    for k in turns:
        blocks = lax.all_gather(blocks, axes[k])
    done = turns[::-1]
    back = [done.index(k) for k in range(len(axes))]
    blocks = blocks.transpose(*back, *range(len(axes), blocks.ndim))
    return blocks.reshape(-1, *array.shape)


def gather_axes(array, axes, turns, dim):
    return in_order(stacked_from(array, axes, turns), dim)


def split_up(array, dim, peers):
    dims = array.shape
    blocks = array.reshape(*dims[:dim], peers, dims[dim] // peers, *dims[dim + 1 :])
    return jnp.moveaxis(blocks, dim, 0)


def summed_on_arrival(array, axis, dim):
    blocks = split_up(array, dim, lax.axis_size(axis))
    arrived = lax.all_to_all(blocks, axis, split_axis=0, concat_axis=0, tiled=True)
    return arrived.astype(jnp.float32).sum(axis=0)


def rms_scale(matrix, gain):
    values = matrix.astype(jnp.float32)
    factor = lax.rsqrt(jnp.mean(values * values, axis=-1, keepdims=True) + 1e-06)
    return values * factor * gain


def causal_taps(mixed, filters):
    length = mixed.shape[-2]
    widths = [(0, 0)] * (mixed.ndim - 2) + [(2, 0), (0, 0)]
    padded = jnp.pad(mixed, widths)
    return (
        filters[0] * padded[..., 0:length, :]
        + filters[1] * padded[..., 1 : length + 1, :]
        + filters[2] * padded[..., 2 : length + 2, :]
    )


def gather_rows(normed):
    return collect(normed, "tp", 0)


def project_in(gathered, stacked):
    return jnp.einsum(
        "td,kdc->ktc",
        gathered,
        lax.all_gather(stacked, FS, axis=1, tiled=True),
        preferred_element_type=jnp.float32,
    )


def collect_out(weight):
    return gather_axes(weight, FS, (0, 1, 2), 1)


def sum_parts(local_cols, weight):
    return summed_on_arrival(
        jnp.dot(local_cols, weight, preferred_element_type=jnp.float32).astype(jnp.bfloat16),
        "tp",
        0,
    )


def on_device(
    tokens, mix_gain, w_bgate, w_cgate, w_value, conv_taps, w_mixout, mlp_gain, w_gate, w_up, w_down
):
    normed = rms_scale(tokens, mix_gain).astype(jnp.bfloat16)
    gathered = gather_rows(normed)
    projected = project_in(gathered, jnp.stack([w_bgate, w_cgate, w_value])).astype(jnp.bfloat16)
    channels = projected.shape[2]
    channel_taps = lax.dynamic_slice_in_dim(conv_taps, lax.axis_index("tp") * channels, channels, 1)
    mixed_in = projected[1].astype(jnp.float32) * projected[2].astype(jnp.float32)
    gated = (projected[0].astype(jnp.float32) * causal_taps(mixed_in, channel_taps)).astype(
        jnp.bfloat16
    )
    residual = tokens.astype(jnp.float32) + sum_parts(gated, collect_out(w_mixout))
    normed_two = rms_scale(residual, mlp_gain).astype(jnp.bfloat16)
    gathered_two = gather_rows(normed_two)
    gate_up = project_in(gathered_two, jnp.stack([w_gate, w_up]))
    hidden = (jax.nn.silu(gate_up[0]) * gate_up[1]).astype(jnp.bfloat16)
    result = residual + 0.5 * sum_parts(hidden, collect_out(w_down))
    return result.astype(jnp.bfloat16)


def solution(mesh):
    finer = Mesh(
        mesh.devices.reshape(mesh.shape["rep"], 2, 4, 4, mesh.shape["tp"]),
        ("rep", "fs_0", "fs_1", "fs_2", "tp"),
    )
    return jax.shard_map(
        on_device,
        mesh=finer,
        in_specs=(
            P(REP_FS_TP, None),
            P(),
            P(FS, "tp"),
            P(FS, "tp"),
            P(FS, "tp"),
            P(),
            P("tp", FS),
            P(),
            P(FS, "tp"),
            P(FS, "tp"),
            P("tp", FS),
        ),
        out_specs=P(REP_FS_TP, None),
        check_vma=False,
    )
```

profile of v0, /device:TPU:1, one launch (start us, length us, event | category | flops | bytes accessed | tf_op | source)
XLA Modules:
  0.0 567.4 jit_solution(2443627094710564930)
XLA Ops:
  6.5 0.0 copy-start.8
  6.5 0.0 copy-start.7
  6.5 0.0 all-gather.17.cloned.1.call-start
  6.5 6.7 %all-gather = bf16[2048,64]{0,1:T(8,128)(2,1)S(1)} all-gather(bf16[1024,64]{0,1:T(8,128)(2,1)} %param.17), channel_id=2, replica_groups=mesh['rep'=2,'fs_0'=2,'fs_1'=4,'fs_2'=4,'tp'=2] {'fs_0'}, dimensions={0}, use_global_device_ids=true | all-gather | bytes 393216 | tf_op jit(solution)/shard_map/all_gather | solution.py:32
  13.3 0.7 copy.27
  14.0 0.0 all-gather.17.cloned.1.call-update
  14.0 0.0 copy-start.4
  14.0 0.0 copy-start.5
  14.0 0.0 all-gather.21.cloned.1.call-start
  14.1 5.9 %all-gather.3 = bf16[2816,64]{0,1:T(8,128)(2,1)S(1)} all-gather(bf16[1408,64]{0,1:T(8,128)(2,1)} %param.21), channel_id=5, replica_groups=mesh['rep'=2,'fs_0'=2,'fs_1'=4,'fs_2'=4,'tp'=2] {'fs_0'}, dimensions={0}, use_global_device_ids=true | all-gather | bytes 540672 | tf_op jit(solution)/shard_map/all_gather | solution.py:32
  20.0 0.8 copy.26
  20.7 0.0 all-gather.21.cloned.1.call-update
  20.7 0.0 all-gather.19.cloned.1.call-start
  20.8 18.1 %all-gather.17.cloned.1.call-done = bf16[8,1024,64]{1,2,0:T(8,128)(2,1)} async-done(((bf16[2,1024,64]{1,2,0:T(8,128)(2,1)}), bf16[8,1024,64]{1,2,0:T(8,128)(2,1)}) %all-gather.17.cloned.1.call-update) | async-done | bytes 1048592 | tf_op jit(solution)/shard_map/all_gather | solution.py:32
  38.9 0.0 all-gather.19.cloned.1.call-update
  39.0 0.0 copy-start.9
  39.0 0.0 all-gather.23.cloned.1.call-start
  39.0 29.2 %all-gather.21.cloned.1.call-done = bf16[8,1408,64]{1,2,0:T(8,128)(2,1)} async-done(((bf16[2,1408,64]{1,2,0:T(8,128)(2,1)}), bf16[8,1408,64]{1,2,0:T(8,128)(2,1)}) %all-gather.21.cloned.1.call-update) | async-done | bytes 1441808 | tf_op jit(solution)/shard_map/all_gather | solution.py:32
  68.3 0.0 all-gather.23.cloned.1.call-update
  68.3 0.0 all-gather.13.cloned.1.call-start
  68.3 0.0 copy-done.8
  68.4 0.0 copy-done.7
  68.4 0.0 copy-done.6
  68.4 0.8 pad_maximum_fusion
  69.2 0.0 all-gather.13.cloned.1.call-update
  69.2 0.0 all-gather.15.cloned.1.call-start
  69.2 0.0 copy-done.4
  69.3 0.0 copy-done.5
  69.3 0.8 pad_maximum_fusion.1
  70.0 0.0 all-gather.15.cloned.1.call-update
  70.1 0.0 copy-done
  70.1 0.4 fusion.1
  70.4 0.0 copy-done.9
  70.5 0.4 fusion.3
  70.8 1.9 broadcast_in_dim.4
  72.7 4.7 all-to-all-start
  77.4 0.9 constant_dynamic-slice_fusion
  78.3 40.2 %all-gather.19.cloned.1.call-done = bf16[16,2,1024,64]{2,3,1,0:T(8,128)(2,1)} async-done(((bf16[4,2,1024,64]{2,3,1,0:T(8,128)(2,1)}), bf16[16,2,1024,64]{2,3,1,0:T(8,128)(2,1)}) %all-gather.19.cloned.1.call-update) | async-done | bytes 4194320 | tf_op jit(solution)/shard_map/all_gather | solution.py:32
  118.5 4.9 copy.19
  123.4 58.3 %all-gather.23.cloned.1.call-done = bf16[16,2,1408,64]{2,3,1,0:T(8,128)(2,1)} async-done(((bf16[4,2,1408,64]{2,3,1,0:T(8,128)(2,1)}), bf16[16,2,1408,64]{2,3,1,0:T(8,128)(2,1)}) %all-gather.23.cloned.1.call-update) | async-done | bytes 5767184 | tf_op jit(solution)/shard_map/all_gather | solution.py:32
  181.7 5.7 %copy.21 = bf16[2,4,4,1408,64]{3,4,2,1,0:T(8,128)(2,1)} copy(bf16[2,4,4,1408,64]{3,4,0,1,2:T(8,128)(2,1)} %bitcast.63) | data formatting | bytes 11534336 | tf_op jit(solution)/shard_map/transpose | solution.py:35
  187.4 0.0 all-to-all-done
  187.4 153.6 %all-gather.13.cloned.1.call-done = bf16[3,2048,1024]{2,1,0:T(8,128)(2,1)} async-done(((bf16[3,64,1024]{2,1,0:T(8,128)(2,1)}), bf16[3,2048,1024]{2,1,0:T(8,128)(2,1)}) %all-gather.13.cloned.1.call-update) | async-done | bytes 12582928 | tf_op jit(solution)/shard_map/all_gather | solution.py:80
  341.0 11.2 %convert_bitcast_fusion = bf16[3,640,1024]{2,1,0:T(8,128)(2,1)S(1)} fusion(bf16[640,2048,1]{1,0,2:T(8,128)(2,1)S(1)} %bitcast.67, bf16[3,2048,1024]{2,1,0:T(8,128)(2,1)} %all-gather.13.cloned.1.call-done), kind=kOutput, calls=%fused_computation.3 | convolution fusion | flops 8055029760 | bytes 19136512 | tf_op jit(solution)/shard_map/td,kdc->ktc/dot_general | solution.py:77
  352.2 0.0 copy-start.3
  352.2 0.5 multiply_bitcast_fusion
  352.8 1.7 copy-done.3
  354.4 3.5 convolution_convert_fusion.1
  357.9 23.8 %all_to_all.20 = bf16[2,320,2048]{2,1,0:T(8,128)(2,1)S(1)} all-to-all(bf16[2,320,2048]{2,1,0:T(8,128)(2,1)S(1)} %bitcast.68), channel_id=1, replica_groups=mesh['rep'=2,'fs_0'=2,'fs_1'=4,'fs_2'=4,'tp'=2] {'tp'}, dimensions={0} | all-to-all | bytes 5242880 | tf_op jit(solution)/shard_map/all_to_all | solution.py:51
  381.7 0.6 convert_reduce_fusion.1
  382.3 0.7 copy-done.1
  383.1 0.5 multiply_reduce_fusion
  383.5 0.2 copy-done.10
  383.7 0.5 multiply_convert_fusion
  384.2 1.9 broadcast_in_dim.5
  386.1 5.4 all-to-all-start.2
  391.5 120.2 %all-gather.15.cloned.1.call-done = bf16[2,2048,1408]{2,1,0:T(8,128)(2,1)} async-done(((bf16[2,64,1408]{2,1,0:T(8,128)(2,1)}), bf16[2,2048,1408]{2,1,0:T(8,128)(2,1)}) %all-gather.15.cloned.1.call-update) | async-done | bytes 11534352 | tf_op jit(solution)/shard_map/all_gather | solution.py:80
  511.6 0.0 all-to-all-done.2
  511.6 13.1 %convolution_bitcast_fusion = f32[2,640,1408]{1,2,0:T(8,128)S(1)} fusion(bf16[2,2048,1408]{2,1,0:T(8,128)(2,1)} %all-gather.15.cloned.1.call-done, bf16[640,2048,1]{1,0,2:T(8,128)(2,1)} %bitcast.21), kind=kOutput, calls=%fused_computation.2 | convolution fusion | flops 7381975040 | bytes 21364736 | tf_op jit(solution)/shard_map/td,kdc->ktc/dot_general | solution.py:77
  524.7 7.0 %convolution_convert_fusion = bf16[640,2048]{1,0:T(8,128)(2,1)S(1)} fusion(bf16[1408,2048]{0,1:T(8,128)(2,1)} %bitcast.64, f32[2,640,1408]{1,2,0:T(8,128)S(1)} %convolution_bitcast_fusion), kind=kOutput, calls=%fused_computation.9 | convolution fusion | flops 3697704960 | bytes 15597568 | tf_op jit(solution)/shard_map/dot_general | solution.py:91
  531.7 25.7 %all_to_all.21 = bf16[2,320,2048]{2,1,0:T(8,128)(2,1)S(1)} all-to-all(bf16[2,320,2048]{2,1,0:T(8,128)(2,1)S(1)} %bitcast.69), channel_id=1, replica_groups=mesh['rep'=2,'fs_0'=2,'fs_1'=4,'fs_2'=4,'tp'=2] {'tp'}, dimensions={0} | all-to-all | bytes 5242880 | tf_op jit(solution)/shard_map/all_to_all | solution.py:51
  557.5 0.6 convert_reduce_fusion
  558.1 0.7 copy-done.2
  558.8 1.8 add_convert_fusion
  (7 shorter events, 0.0 us)
Async XLA Ops:
  6.5 61.8 %copy-start.8 = (bf16[64,1024]{1,0:T(8,128)(2,1)S(1)}, bf16[64,1024]{1,0:T(8,128)(2,1)}, u32[]{:S(2)}) copy-start(bf16[64,1024]{1,0:T(8,128)(2,1)} %param.13) | copy-start | bytes 393220
  6.5 61.8 %copy-start.7 = (bf16[64,1024]{1,0:T(8,128)(2,1)S(1)}, bf16[64,1024]{1,0:T(8,128)(2,1)}, u32[]{:S(2)}) copy-start(bf16[64,1024]{1,0:T(8,128)(2,1)} %param.14) | copy-start | bytes 393220
  6.5 61.8 %copy-start.6 = (bf16[64,1024]{1,0:T(8,128)(2,1)S(1)}, bf16[64,1024]{1,0:T(8,128)(2,1)}, u32[]{:S(2)}) copy-start(bf16[64,1024]{1,0:T(8,128)(2,1)} %param.15) | copy-start | bytes 393220
  6.5 32.4 %all-gather.17.cloned.1.call-start = ((), (), s32[]{:S(2)}) async-start(), calls=%async_computation.6 | async-start | bytes 1310720 | tf_op jit(solution)/shard_map/all_gather | solution.py:32
  14.0 55.2 %copy-start.4 = (bf16[64,1408]{1,0:T(8,128)(2,1)S(1)}, bf16[64,1408]{1,0:T(8,128)(2,1)}, u32[]{:S(2)}) copy-start(bf16[64,1408]{1,0:T(8,128)(2,1)} %param.20) | copy-start | bytes 540676
  14.0 55.2 %copy-start.5 = (bf16[64,1408]{1,0:T(8,128)(2,1)S(1)}, bf16[64,1408]{1,0:T(8,128)(2,1)}, u32[]{:S(2)}) copy-start(bf16[64,1408]{1,0:T(8,128)(2,1)} %param.19) | copy-start | bytes 540676
  14.0 54.2 %all-gather.21.cloned.1.call-start = ((), (), s32[]{:S(2)}) async-start(), calls=%async_computation.8 | async-start | bytes 1802240 | tf_op jit(solution)/shard_map/all_gather | solution.py:32
  20.7 49.4 %copy-start = (bf16[320,2048]{1,0:T(8,128)(2,1)S(1)}, bf16[320,2048]{1,0:T(8,128)(2,1)}, u32[]{:S(2)}) copy-start(bf16[320,2048]{1,0:T(8,128)(2,1)} %param.11) | copy-start | bytes 3932164
  20.7 97.8 %all-gather.19.cloned.1.call-start = ((), (), s32[]{:S(2)}) async-start(), calls=%async_computation.7 | async-start | bytes 5242880 | tf_op jit(solution)/shard_map/all_gather | solution.py:32
  39.0 31.5 %copy-start.9 = (f32[2048]{0:T(1024)S(1)}, f32[2048]{0:T(1024)}, u32[]{:S(2)}) copy-start(f32[2048]{0:T(1024)} %param.12) | copy-start | bytes 24580
  39.0 142.7 %all-gather.23.cloned.1.call-start = ((), (), s32[]{:S(2)}) async-start(), calls=%async_computation.9 | async-start | bytes 7208960 | tf_op jit(solution)/shard_map/all_gather | solution.py:32
  68.3 272.7 %all-gather.13.cloned.1.call-start = ((), (), s32[]{:S(2)}) async-start(), calls=%async_computation.4 | async-start | bytes 12976128 | tf_op jit(solution)/shard_map/all_gather | solution.py:80
  69.2 442.4 %all-gather.15.cloned.1.call-start = ((), (), s32[]{:S(2)}) async-start(), calls=%async_computation.5 | async-start | bytes 11894784 | tf_op jit(solution)/shard_map/all_gather | solution.py:80
  72.7 114.7 %all-to-all-start = ((bf16[2,320,2048]{2,1,0:T(8,128)(2,1)}), bf16[2,320,2048]{2,1,0:T(8,128)(2,1)S(1)}, u32[]{:S(2)}, u32[]{:S(2)}) async-start(bf16[2,320,2048]{2,1,0:T(8,128)(2,1)} %broadcast_in_dim.4), calls=%async_computation | async-start | bytes 5242880 | tf_op jit(solution)/shard_map/all_to_all | solution.py:13
  352.2 2.2 copy-start.3
  381.7 1.3 copy-start.1
  383.0 0.7 copy-start.10
  386.1 125.5 %all-to-all-start.2 = ((bf16[2,320,2048]{2,1,0:T(8,128)(2,1)}), bf16[2,320,2048]{2,1,0:T(8,128)(2,1)}, u32[]{:S(2)}, u32[]{:S(2)}) async-start(bf16[2,320,2048]{2,1,0:T(8,128)(2,1)} %broadcast_in_dim.5), calls=%async_computation.2 | async-start | bytes 5242880 | tf_op jit(solution)/shard_map/all_to_all | solution.py:13
  557.5 1.3 copy-start.2
Sparse Core Ops, SparseCore 0:
  14.1 24.7 all-gather.16
  40.6 27.6 all-gather.20
  69.9 48.5 all-gather.18
  120.0 61.5 all-gather.22
  183.1 157.7 all-gather.12
  342.5 169.0 all-gather.14
where the time goes:
time: 568 us; the launch traced here: 567 us
  waiting for transfers between devices  420 us (74%)
  blocking collectives  62.1 us (11%)
  matrix products  34.9 us (6%)
  local copies, waits for them, and re-layouts  20.1 us (4%)
  between operations  13.6 us (2%)
  starting transfers between devices  10.3 us (2%)
  other arithmetic  6.69 us (1%)
    all_gather x2, waiting for transfers between devices, project_in(): lax.all_gather(stacked, FS, axis=1, tiled=True)  274 us
    all_gather x4, waiting for transfers between devices, stacked_from(): blocks = lax.all_gather(blocks, axes[k])  146 us
    all_to_all x2, blocking collectives, summed_on_arrival(): lax.all_to_all(blocks, axis, split_axis=0, concat_axis=0, tiled=True)  49.5 us
    dot_general x2, matrix products, project_in(): jnp.einsum('td,kdc->ktc', gathered, lax.all_gather(stacked, FS, axis=1, t...  24.3 us
    all_gather x2, blocking collectives, stacked_from(): blocks = lax.all_gather(blocks, axes[k])  12.6 us
  transfers between devices with their start and end apart: 8, of which 6 were waited for; matrix products, arithmetic and copies ran while one was open for 6% of the time, Pallas kernels for 0%

commit v1 on v0

--- a/solution.py
+++ b/solution.py
@@ -77,7 +77,7 @@
     return jnp.einsum(
         "td,kdc->ktc",
         gathered,
-        lax.all_gather(stacked, FS, axis=1, tiled=True),
+        jnp.concatenate(lax.all_to_all(jnp.stack([stacked] * lax.axis_size(FS)), FS, 0, 0), axis=1),
         preferred_element_type=jnp.float32,
     )
 

time: 568 us -> 563 us (level)
  waiting for transfers between devices: 420 us -> 321 us
  starting transfers between devices: 10.3 us -> 46.4 us
  local copies, waits for them, and re-layouts: 20.1 us -> 49.6 us
  blocking collectives: 62.1 us -> 87.8 us
    all_gather x2 -> x0, waiting for transfers between devices: 274 us -> none  [project_in(): lax.all_gather(stacked, FS, axis=1, tiled=True)]
    all_gather x4, waiting for transfers between devices: 146 us -> 320 us  [stacked_from(): blocks = lax.all_gather(blocks, axes[k])]
    all_gather x2, blocking collectives: 12.6 us -> 69.9 us  [stacked_from(): blocks = lax.all_gather(blocks, axes[k])]
    all_to_all x0 -> x2, starting transfers between devices: none -> 40.5 us  [project_in(): lax.all_to_all(jnp.stack([stacked] * lax.axis_size(FS)), FS, 0, 0)]
    all_to_all x2, blocking collectives: 49.5 us -> 11.5 us  [summed_on_arrival(): lax.all_to_all(blocks, axis, split_axis=0, concat_axis=0, tiled=True)]
    another operation x0 -> x2, local copies, waits for them, and re-layouts: none -> 12 us  [project_in(): jnp.stack([stacked] * lax.axis_size(FS))]
    reshape x0 -> x1, local copies, waits for them, and re-layouts: none -> 10.7 us  [project_in(): jnp.concatenate(lax.all_to_all(jnp.stack([stacked] * lax.axis_size(FS)),...]
    all_to_all x0 -> x1, local copies, waits for them, and re-layouts: none -> 9.97 us  [project_in(): lax.all_to_all(jnp.stack([stacked] * lax.axis_size(FS)), FS, 0, 0)]
  transfers between devices with their start and end apart: 8 -> 7, of which waited for: 6 -> 3; matrix products, arithmetic and copies ran while one was open for 6% -> 7% of each run, Pallas kernels for 0% -> 0%
where the time goes in v1:
time: 563 us; the launch traced here: 559 us
  waiting for transfers between devices  321 us (57%)
  blocking collectives  87.8 us (16%)
  local copies, waits for them, and re-layouts  49.6 us (9%)
  starting transfers between devices  46.4 us (8%)
  matrix products  34.9 us (6%)
  between operations  13.4 us (2%)
  other arithmetic  6.21 us (1%)
    all_gather x4, waiting for transfers between devices, stacked_from(): blocks = lax.all_gather(blocks, axes[k])  320 us
    all_gather x2, blocking collectives, stacked_from(): blocks = lax.all_gather(blocks, axes[k])  69.9 us
    all_to_all x2, starting transfers between devices, project_in(): lax.all_to_all(jnp.stack([stacked] * lax.axis_size(FS)), FS, 0, 0)  40.5 us
    dot_general x2, matrix products, project_in(): jnp.einsum('td,kdc->ktc', gathered, jnp.concatenate(lax.all_to_all(jnp.st...  23.6 us
    another operation x2, local copies, waits for them, and re-layouts, project_in(): jnp.stack([stacked] * lax.axis_size(FS))  12 us
    all_to_all x2, blocking collectives, summed_on_arrival(): lax.all_to_all(blocks, axis, split_axis=0, concat_axis=0, tiled=True)  11.5 us
    dot_general x2, matrix products, sum_parts(): jnp.dot(local_cols, weight, preferred_element_type=jnp.float32)  11.3 us
  transfers between devices with their start and end apart: 7, of which 3 were waited for; matrix products, arithmetic and copies ran while one was open for 7% of the time, Pallas kernels for 0%

profile of v1, /device:TPU:1, one launch (start us, length us, event | category | flops | bytes accessed | tf_op | source)
XLA Modules:
  0.0 559.3 jit_solution(10694746672683173550)
XLA Ops:
  6.5 1.0 pad_maximum_fusion.1
  7.6 5.8 %stack.26 = bf16[32,2,64,1408]{3,2,1,0:T(8,128)(2,1)} broadcast(bf16[2,64,1408]{2,1,0:T(8,128)(2,1)S(1)} %pad_maximum_fusion.1), dimensions={1,2,3} | broadcast | bytes 11894784 | tf_op jit(solution)/shard_map/stack | solution.py:80
  13.4 9.5 %all-to-all-start.3 = ((bf16[32,2,64,1408]{3,2,1,0:T(8,128)(2,1)}), bf16[32,2,64,1408]{3,2,1,0:T(8,128)(2,1)}, u32[]{:S(2)}, u32[]{:S(2)}) async-start(bf16[32,2,64,1408]{3,2,1,0:T(8,128)(2,1)} %stack.26), calls=%async_computation.3 | async-start | bytes 23068672 | tf_op jit(solution)/shard_map/all_to_all | solution.py:80
  22.9 0.0 copy-start.4
  22.9 0.0 copy-start.5
  22.9 0.0 copy-start.6
  22.9 0.0 all-gather.11.cloned.1.call-start
  23.0 0.0 copy-done.3
  23.0 64.3 %all-gather = bf16[2048,64]{0,1:T(8,128)(2,1)S(1)} all-gather(bf16[1024,64]{0,1:T(8,128)(2,1)S(1)} %copy-done.3), channel_id=2, replica_groups=mesh['rep'=2,'fs_0'=2,'fs_1'=4,'fs_2'=4,'tp'=2] {'fs_0'}, dimensions={0}, use_global_device_ids=true | all-gather | bytes 393216 | tf_op jit(solution)/shard_map/all_gather | solution.py:32
  87.3 0.7 copy.37
  88.0 0.0 all-gather.11.cloned.1.call-update
  88.1 0.0 all-gather.15.cloned.1.call-start
  88.1 0.0 copy-done.2
  88.1 5.6 all-gather.3
  93.7 0.8 copy.36
  94.5 0.0 all-gather.15.cloned.1.call-update
  94.5 0.0 all-gather.13.cloned.1.call-start
  94.6 98.7 %all-gather.11.cloned.1.call-done = bf16[8,1024,64]{1,2,0:T(8,128)(2,1)} async-done(((bf16[2,1024,64]{1,2,0:T(8,128)(2,1)}), bf16[8,1024,64]{1,2,0:T(8,128)(2,1)}) %all-gather.11.cloned.1.call-update) | async-done | bytes 1048592 | tf_op jit(solution)/shard_map/all_gather | solution.py:32
  193.2 0.0 all-gather.13.cloned.1.call-update
  193.2 0.0 copy-done.4
  193.2 0.0 copy-done.5
  193.3 0.0 all-to-all-done.3
  193.3 6.1 %stack.22 = bf16[32,3,64,1024]{3,2,1,0:T(8,128)(2,1)} broadcast(bf16[3,64,1024]{2,1,0:T(8,128)(2,1)S(1)} %pad_maximum_fusion), dimensions={1,2,3} | broadcast | bytes 12976128 | tf_op jit(solution)/shard_map/stack | solution.py:80
  199.5 31.1 %all-to-all-start = ((bf16[32,3,64,1024]{3,2,1,0:T(8,128)(2,1)}), bf16[32,3,64,1024]{3,2,1,0:T(8,128)(2,1)}, u32[]{:S(2)}, u32[]{:S(2)}) async-start(bf16[32,3,64,1024]{3,2,1,0:T(8,128)(2,1)} %stack.22), calls=%async_computation | async-start | bytes 25165824 | tf_op jit(solution)/shard_map/all_to_all | solution.py:80
  230.6 0.0 copy-start.7
  230.6 0.0 all-gather.17.cloned.1.call-start
  230.6 0.0 all-gather.15.cloned.1.call-done
  230.7 0.5 all-gather.17.cloned.1.call-update
  231.2 0.9 constant_dynamic-slice_fusion
  232.1 0.4 fusion.1
  232.5 0.4 fusion.3
  232.8 118.6 %all-gather.13.cloned.1.call-done = bf16[16,2,1024,64]{2,3,1,0:T(8,128)(2,1)} async-done(((bf16[4,2,1024,64]{2,3,1,0:T(8,128)(2,1)}), bf16[16,2,1024,64]{2,3,1,0:T(8,128)(2,1)}) %all-gather.13.cloned.1.call-update) | async-done | bytes 4194320 | tf_op jit(solution)/shard_map/all_gather | solution.py:32
  351.4 4.9 copy.26
  356.3 103.2 %all-gather.17.cloned.1.call-done = bf16[16,2,1408,64]{2,3,1,0:T(8,128)(2,1)} async-done(((bf16[4,2,1408,64]{2,3,1,0:T(8,128)(2,1)}), bf16[16,2,1408,64]{2,3,1,0:T(8,128)(2,1)}) %all-gather.17.cloned.1.call-update) | async-done | bytes 5767184 | tf_op jit(solution)/shard_map/all_gather | solution.py:32
  459.5 5.7 %copy.30 = bf16[2,4,4,1408,64]{3,4,2,1,0:T(8,128)(2,1)} copy(bf16[2,4,4,1408,64]{3,4,0,1,2:T(8,128)(2,1)} %bitcast.75) | data formatting | bytes 11534336 | tf_op jit(solution)/shard_map/transpose | solution.py:35
  465.2 10.0 %copy.27 = bf16[32,2,64,1408]{3,2,0,1:T(8,128)(2,1)} copy(bf16[32,2,64,1408]{3,2,1,0:T(8,128)(2,1)} %all-to-all-done.3) | data formatting | bytes 23068672 | tf_op jit(solution)/shard_map/all_to_all | solution.py:80
  475.1 0.0 all-to-all-done
  475.1 1.9 broadcast_in_dim.4
  477.1 5.7 %all-to-all-start.1 = ((bf16[2,320,2048]{2,1,0:T(8,128)(2,1)}), bf16[2,320,2048]{2,1,0:T(8,128)(2,1)}, u32[]{:S(2)}, u32[]{:S(2)}) async-start(bf16[2,320,2048]{2,1,0:T(8,128)(2,1)} %broadcast_in_dim.4), calls=%async_computation.1 | async-start | bytes 5242880 | tf_op jit(solution)/shard_map/all_to_all | solution.py:13
  482.8 10.7 %copy.24 = bf16[3,32,64,1024]{3,2,1,0:T(8,128)(2,1)} copy(bf16[3,32,64,1024]{3,2,0,1:T(8,128)(2,1)} %bitcast.3) | data formatting | bytes 25165824 | tf_op jit(solution)/shard_map/reshape | solution.py:80
  493.5 0.0 all-to-all-done.1
  493.5 12.0 %convert_bitcast_fusion = bf16[3,640,1024]{2,1,0:T(8,128)(2,1)S(1)} fusion(bf16[640,2048,1]{1,0,2:T(8,128)(2,1)} %bitcast.6, bf16[3,2048,1024]{2,1,0:T(8,128)(2,1)} %bitcast.68), kind=kOutput, calls=%fused_computation.3 | convolution fusion | flops 8055029760 | bytes 19136512 | tf_op jit(solution)/shard_map/td,kdc->ktc/dot_general | solution.py:77
  505.5 0.0 copy-start.1
  505.6 0.5 multiply_bitcast_fusion
  506.1 1.7 copy-done.1
  507.7 3.5 convolution_convert_fusion.1
  511.2 5.7 %all_to_all.30 = bf16[2,320,2048]{2,1,0:T(8,128)(2,1)S(1)} all-to-all(bf16[2,320,2048]{2,1,0:T(8,128)(2,1)S(1)} %bitcast.78), channel_id=1, replica_groups=mesh['rep'=2,'fs_0'=2,'fs_1'=4,'fs_2'=4,'tp'=2] {'tp'}, dimensions={0} | all-to-all | bytes 5242880 | tf_op jit(solution)/shard_map/all_to_all | solution.py:51
  516.9 0.6 convert_reduce_fusion.1
  517.5 0.0 slice-start.1
  517.5 0.5 multiply_reduce_fusion
  518.0 0.0 copy-done.8
  518.0 0.5 multiply_convert_fusion
  518.5 0.0 slice-start.2
  518.5 0.3 broadcast_in_dim.5
  518.8 0.0 slice-start.3
  518.8 6.4 %all_to_all.31 = bf16[2,320,2048]{2,1,0:T(8,128)(2,1)S(1)} all-to-all(bf16[2,320,2048]{2,1,0:T(8,128)(2,1)S(1)} %broadcast_in_dim.5), channel_id=1, replica_groups=mesh['rep'=2,'fs_0'=2,'fs_1'=4,'fs_2'=4,'tp'=2] {'tp'}, dimensions={0} | all-to-all | bytes 5242880 | tf_op jit(solution)/shard_map/all_to_all | solution.py:13
  525.2 0.0 slice-done
  525.2 0.0 slice-start.4
  525.2 11.5 %convolution_bitcast_fusion = f32[2,640,1408]{1,2,0:T(8,128)} fusion(bf16[2,2048,1408]{2,1,0:T(8,128)(2,1)S(1)} %bitcast.71, bf16[640,2048,1]{1,0,2:T(8,128)(2,1)S(1)} %bitcast.79), kind=kOutput, calls=%fused_computation.2 | convolution fusion | flops 7381975040 | bytes 21364736 | tf_op jit(solution)/shard_map/td,kdc->ktc/dot_general | solution.py:77
  536.8 0.0 slice-done.3
  536.8 7.8 %convolution_convert_fusion = bf16[640,2048]{1,0:T(8,128)(2,1)S(1)} fusion(bf16[1408,2048]{0,1:T(8,128)(2,1)S(1)} %bitcast.74, f32[2,640,1408]{1,2,0:T(8,128)} %convolution_bitcast_fusion), kind=kOutput, calls=%fused_computation.9 | convolution fusion | flops 3697704960 | bytes 15597568 | tf_op jit(solution)/shard_map/dot_general | solution.py:91
  544.6 5.8 %all_to_all.32 = bf16[2,320,2048]{2,1,0:T(8,128)(2,1)S(1)} all-to-all(bf16[2,320,2048]{2,1,0:T(8,128)(2,1)S(1)} %bitcast.80), channel_id=1, replica_groups=mesh['rep'=2,'fs_0'=2,'fs_1'=4,'fs_2'=4,'tp'=2] {'tp'}, dimensions={0} | all-to-all | bytes 5242880 | tf_op jit(solution)/shard_map/all_to_all | solution.py:51
  550.4 0.6 convert_reduce_fusion
  551.0 1.8 add_convert_fusion
  (16 shorter events, 0.1 us)
Async XLA Ops:
  13.4 9.6 %copy-start.3 = (bf16[1024,64]{0,1:T(8,128)(2,1)S(1)}, bf16[1024,64]{0,1:T(8,128)(2,1)}, u32[]{:S(2)}) copy-start(bf16[1024,64]{0,1:T(8,128)(2,1)} %param.17) | copy-start | bytes 393220
  13.4 74.7 %copy-start.2 = (bf16[1408,64]{0,1:T(8,128)(2,1)S(1)}, bf16[1408,64]{0,1:T(8,128)(2,1)}, u32[]{:S(2)}) copy-start(bf16[1408,64]{0,1:T(8,128)(2,1)} %param.21) | copy-start | bytes 540676
  13.4 179.9 %all-to-all-start.3 = ((bf16[32,2,64,1408]{3,2,1,0:T(8,128)(2,1)}), bf16[32,2,64,1408]{3,2,1,0:T(8,128)(2,1)}, u32[]{:S(2)}, u32[]{:S(2)}) async-start(bf16[32,2,64,1408]{3,2,1,0:T(8,128)(2,1)} %stack.26), calls=%async_computation.3 | async-start | bytes 23068672 | tf_op jit(solution)/shard_map/all_to_all | solution.py:80
  22.9 170.4 %copy-start.4 = (bf16[64,1024]{1,0:T(8,128)(2,1)S(1)}, bf16[64,1024]{1,0:T(8,128)(2,1)}, u32[]{:S(2)}) copy-start(bf16[64,1024]{1,0:T(8,128)(2,1)} %param.15) | copy-start | bytes 393220
  22.9 170.4 %copy-start.5 = (bf16[64,1024]{1,0:T(8,128)(2,1)S(1)}, bf16[64,1024]{1,0:T(8,128)(2,1)}, u32[]{:S(2)}) copy-start(bf16[64,1024]{1,0:T(8,128)(2,1)} %param.14) | copy-start | bytes 393220
  22.9 170.3 %copy-start.6 = (bf16[64,1024]{1,0:T(8,128)(2,1)S(1)}, bf16[64,1024]{1,0:T(8,128)(2,1)}, u32[]{:S(2)}) copy-start(bf16[64,1024]{1,0:T(8,128)(2,1)} %param.13) | copy-start | bytes 393220
  22.9 170.3 %all-gather.11.cloned.1.call-start = ((), (), s32[]{:S(2)}) async-start(), calls=%async_computation.6 | async-start | bytes 1310720 | tf_op jit(solution)/shard_map/all_gather | solution.py:32
  88.1 142.6 %all-gather.15.cloned.1.call-start = ((), (), s32[]{:S(2)}) async-start(), calls=%async_computation.8 | async-start | bytes 1802240 | tf_op jit(solution)/shard_map/all_gather | solution.py:32
  94.5 256.9 %all-gather.13.cloned.1.call-start = ((), (), s32[]{:S(2)}) async-start(), calls=%async_computation.7 | async-start | bytes 5242880 | tf_op jit(solution)/shard_map/all_gather | solution.py:32
  199.5 32.6 %copy-start = (bf16[320,2048]{1,0:T(8,128)(2,1)S(1)}, bf16[320,2048]{1,0:T(8,128)(2,1)}, u32[]{:S(2)}) copy-start(bf16[320,2048]{1,0:T(8,128)(2,1)} %param.11) | copy-start | bytes 3932164
  199.5 275.7 %all-to-all-start = ((bf16[32,3,64,1024]{3,2,1,0:T(8,128)(2,1)}), bf16[32,3,64,1024]{3,2,1,0:T(8,128)(2,1)}, u32[]{:S(2)}, u32[]{:S(2)}) async-start(bf16[32,3,64,1024]{3,2,1,0:T(8,128)(2,1)} %stack.22), calls=%async_computation | async-start | bytes 25165824 | tf_op jit(solution)/shard_map/all_to_all | solution.py:80
  230.6 1.9 copy-start.7
  230.6 228.9 %all-gather.17.cloned.1.call-start = ((), (), s32[]{:S(2)}) async-start(), calls=%async_computation.9 | async-start | bytes 7208960 | tf_op jit(solution)/shard_map/all_gather | solution.py:32
  477.1 16.4 %all-to-all-start.1 = ((bf16[2,320,2048]{2,1,0:T(8,128)(2,1)}), bf16[2,320,2048]{2,1,0:T(8,128)(2,1)}, u32[]{:S(2)}, u32[]{:S(2)}) async-start(bf16[2,320,2048]{2,1,0:T(8,128)(2,1)} %broadcast_in_dim.4), calls=%async_computation.1 | async-start | bytes 5242880 | tf_op jit(solution)/shard_map/all_to_all | solution.py:13
  505.5 2.2 copy-start.1
  516.9 1.1 copy-start.8
  516.9 8.3 %slice-start = ((s8[11534336]{0:T(1024)(128)(4,1)}), s8[4194304]{0:T(1024)(128)(4,1)S(1)}, s32[]{:S(2)}) async-start(s8[11534336]{0:T(1024)(128)(4,1)} %bitcast.69), calls=%async_computation.10 | async-start | bytes 8388608
  517.5 7.7 %slice-start.1 = ((s8[11534336]{0:T(1024)(128)(4,1)}), s8[4194304]{0:T(1024)(128)(4,1)S(1)}, s32[]{:S(2)}) async-start(s8[11534336]{0:T(1024)(128)(4,1)} %bitcast.69), calls=%async_computation.11 | async-start | bytes 8388608
  518.5 6.7 %slice-start.2 = ((s8[11534336]{0:T(1024)(128)(4,1)}), s8[3145728]{0:T(1024)(128)(4,1)S(1)}, s32[]{:S(2)}) async-start(s8[11534336]{0:T(1024)(128)(4,1)} %bitcast.69), calls=%async_computation.12 | async-start | bytes 6291456
  518.8 17.9 %slice-start.3 = ((s8[5767168]{0:T(1024)(128)(4,1)}), s8[4194304]{0:T(1024)(128)(4,1)S(1)}, s32[]{:S(2)}) async-start(s8[5767168]{0:T(1024)(128)(4,1)} %bitcast.72), calls=%async_computation.13 | async-start | bytes 8388608
  525.2 11.6 %slice-start.4 = ((s8[5767168]{0:T(1024)(128)(4,1)}), s8[1572864]{0:T(1024)(128)(4,1)S(1)}, s32[]{:S(2)}) async-start(s8[5767168]{0:T(1024)(128)(4,1)} %bitcast.72), calls=%async_computation.14 | async-start | bytes 3145728
Sparse Core Ops, SparseCore 0:
  88.2 104.9 all-gather.10
  194.9 25.2 all-gather.14
  221.8 129.5 all-gather.12
  353.0 106.4 all-gather.16
